TPU v7x, 32 devices: a whole 2x2x4 slice. The times are simulated.
32 devices in a mesh: sp: 8 (over z, y), dp: 4 (over x, core).
Axes of the slice: x: 2, y: 2, z: 4, core: 2. Of those that a mesh axis runs over, the one named last changes fastest.
Arguments:
- resid: bfloat16 [4, 2048, 2048], P('dp', 'sp'), may hold values from -6 to 6
- mixer_inputs: bfloat16 [4, 2048, 4096], P('dp', 'sp'), may hold values from -6 to 6
- output_gate: bfloat16 [4, 2048, 4096], P('dp', 'sp'), may hold values from -6 to 6
- write_rows_input: bfloat16 [4, 2048, 256], P('dp', 'sp'), may hold values from -6 to 6
- read_rows_input: bfloat16 [4, 2048, 256], P('dp', 'sp'), may hold values from -6 to 6
- step_size_logits: bfloat16 [4, 2048, 64, 2], P('dp', 'sp'), may hold values from -5 to 5
- extra_log_decay: bfloat16 [4, 2048, 64, 2], P('dp', 'sp'), may hold values from -0.7 to 0
- mixer_conv_taps: bfloat16 [5, 4096], P(None, 'sp'), may hold values from -2.5 to 2.5
- write_conv_taps: bfloat16 [5, 256], replicated, may hold values from -2.5 to 2.5
- read_conv_taps: bfloat16 [5, 256], replicated, may hold values from -2.5 to 2.5
- step_size_bias: float32 [64, 2], P('sp'), may hold values from -20 to -3
- decay_speed: float32 [64, 2], P('sp'), may hold values from 1 to 16
- grouped_norm_gain: float32 [4096], replicated, may hold values from 0.1 to 1.9
- output_matrix: bfloat16 [4096, 2048], P(None, 'dp'), may hold values from -0.09375 to 0.09375
- output_gain: float32 [2048], replicated, may hold values from 0.1 to 1.9
- feedforward_gain: float32 [2048], replicated, may hold values from 0.1 to 1.9
- routes: int32 [4, 2048, 2], P('dp', 'sp'), may hold values from 0 to 7, all different within a row; in each aligned block of 256 rows (0 to 255, 256 to 511, ..., all dimensions but the last counted through in order) at most 96 rows name the same one
- route_weights: float32 [4, 2048, 2], P('dp', 'sp'), may hold values from 0.1 to 1
- expert_gate_weight: bfloat16 [8, 2048, 1024], P('sp'), may hold values from -0.125 to 0.125
- expert_up_weight: bfloat16 [8, 2048, 1024], P('sp'), may hold values from -0.125 to 0.125
- expert_down_weight: bfloat16 [8, 1024, 2048], P('sp'), may hold values from -0.1875 to 0.1875
- expert_sum_gain: float32 [2048], replicated, may hold values from 0.1 to 1.9
Outputs:
- mixed_out: bfloat16 [4, 2048, 2048], P('dp', 'sp')
Inputs may be any that keep to these rules, and one draw needn't show every extreme that they name: `routes`: each token names 2 different experts; the 256 positions of one device name one expert at most 96 times, a bound that some block reaches.
All inputs are finite; a program needn't handle non-finite values.
Results may differ from a plain program's by a relative error of at most 0.012.
Values may be sent and summed in bfloat16 or wider, within the bound.
A program may use at most 128 MiB of HBM per device.

v0:
```python
import jax
import jax.numpy as jnp
from jax import lax
from jax.sharding import PartitionSpec as P

D = 2048
HEADS = 64
HEAD_DIM = 64
GROUPS = 2
STATE = 128
BLOCK = 128
TOPK = 2
INNER = 4096
EPS = 1e-06


def rms_scale(values, scale_gain):
    return values * lax.rsqrt(jnp.mean(values * values, axis=-1, keepdims=True) + EPS) * scale_gain


def centred_conv(values, kernel):
    span_len = kernel.shape[0]
    half_span = span_len // 2
    length = values.shape[0]
    padded = jnp.pad(values.astype(jnp.float32), ((half_span, half_span), (0, 0)))
    summed = jnp.zeros(values.shape, jnp.float32)
    for offset in range(span_len):
        summed = summed + padded[offset : offset + length] * kernel[offset].astype(jnp.float32)
    return jax.nn.silu(summed).astype(jnp.bfloat16)


def block_pass(inputs, writes, read_rows, head_step_sizes, logarithm_decay):
    length = inputs.shape[0]
    blocks = length // BLOCK
    inp_block = inputs.reshape(blocks, BLOCK, -1)
    wr_block = writes.reshape(blocks, BLOCK, -1)
    rd_block = read_rows.reshape(blocks, BLOCK, -1)
    step_blk = head_step_sizes.reshape(blocks, BLOCK)
    cumulative = jnp.cumsum(logarithm_decay.reshape(blocks, BLOCK), axis=1)
    lower_tri = jnp.tril(jnp.ones((BLOCK, BLOCK), dtype=bool))
    spread = cumulative[:, :, None] - cumulative[:, None, :]
    in_block = jnp.where(lower_tri, jnp.exp(jnp.where(lower_tri, spread, 0.0)), 0.0)
    scores = jnp.einsum("cln,csn->cls", rd_block, wr_block, preferred_element_type=jnp.float32)
    weights = (scores * in_block * step_blk[:, None, :]).astype(jnp.bfloat16)
    within = jnp.einsum("cls,csp->clp", weights, inp_block, preferred_element_type=jnp.float32)
    to_end = jnp.exp(cumulative[:, -1:] - cumulative) * step_blk
    scaled = (wr_block.astype(jnp.float32) * to_end[:, :, None]).astype(jnp.bfloat16)
    states = jnp.einsum("csn,csp->cnp", scaled, inp_block, preferred_element_type=jnp.float32)
    totals = cumulative[:, -1]
    through = jnp.cumsum(totals)
    preceding = through - totals
    strict = jnp.tril(jnp.ones((blocks, blocks), dtype=bool), -1)
    carry_mat = jnp.where(
        strict, jnp.exp(jnp.where(strict, preceding[:, None] - through[None, :], 0.0)), 0.0
    )
    entering = jnp.dot(carry_mat, states.reshape(blocks, -1), precision=lax.Precision.HIGHEST)
    entering = entering.reshape(states.shape).astype(jnp.bfloat16)
    carried = (
        jnp.einsum("cln,cnp->clp", rd_block, entering, preferred_element_type=jnp.float32)
        * jnp.exp(cumulative)[:, :, None]
    )
    return (within + carried).reshape(length, -1)


def both_ways(inputs, writes, read_rows, head_step_sizes, logarithm_decay):
    forward = block_pass(inputs, writes, read_rows, head_step_sizes[:, 0], logarithm_decay[:, 0])
    backward = block_pass(
        jnp.flip(inputs, 0),
        jnp.flip(writes, 0),
        jnp.flip(read_rows, 0),
        jnp.flip(head_step_sizes[:, 1], 0),
        jnp.flip(logarithm_decay[:, 1], 0),
    )
    return forward + jnp.flip(backward, 0)


def head_result(packed_head):
    return both_ways(*packed_head).astype(jnp.bfloat16)


def local(
    resid,
    mixer_inputs,
    output_gate,
    write_rows_input,
    read_rows_input,
    step_size_logits,
    extra_log_decay,
    mixer_conv_taps,
    write_conv_taps,
    read_conv_taps,
    step_size_bias,
    decay_speed,
    grouped_norm_gain,
    output_matrix,
    output_gain,
    feedforward_gain,
    routes,
    route_weights,
    expert_gate_weight,
    expert_up_weight,
    expert_down_weight,
    expert_sum_gain,
):
    tok_rows = mixer_inputs.shape[1]
    local_heads = step_size_bias.shape[0]
    per_group = HEADS // GROUPS
    first_head = lax.axis_index("sp") * local_heads
    group_id = first_head // per_group
    heads_x = mixer_inputs[0].reshape(tok_rows, HEADS, HEAD_DIM)
    shifted_inputs, shifted_step_pre, shifted_extra_decay = (
        lax.all_to_all(heads_x, "sp", split_axis=1, concat_axis=0, tiled=True),
        lax.all_to_all(step_size_logits[0], "sp", split_axis=1, concat_axis=0, tiled=True),
        lax.all_to_all(extra_log_decay[0], "sp", split_axis=1, concat_axis=0, tiled=True),
    )
    seq_len = shifted_inputs.shape[0]
    whole_write, whole_read = (
        lax.all_gather(write_rows_input[0], "sp", axis=0, tiled=True),
        lax.all_gather(read_rows_input[0], "sp", axis=0, tiled=True),
    )
    col_start = group_id * STATE
    write_act = centred_conv(
        lax.dynamic_slice_in_dim(whole_write, col_start, STATE, 1),
        lax.dynamic_slice_in_dim(write_conv_taps, col_start, STATE, 1),
    )
    read_act = centred_conv(
        lax.dynamic_slice_in_dim(whole_read, col_start, STATE, 1),
        lax.dynamic_slice_in_dim(read_conv_taps, col_start, STATE, 1),
    )
    write_heads = jnp.broadcast_to(write_act[:, None, :], (seq_len, local_heads, STATE))
    read_heads = jnp.broadcast_to(read_act[:, None, :], (seq_len, local_heads, STATE))
    x_act = centred_conv(shifted_inputs.reshape(seq_len, local_heads * HEAD_DIM), mixer_conv_taps)
    x_act = x_act.reshape(seq_len, local_heads, HEAD_DIM)
    head_step_sizes = jax.nn.softplus(shifted_step_pre.astype(jnp.float32) + step_size_bias)
    logarithm_decay = shifted_extra_decay.astype(jnp.float32) - decay_speed * head_step_sizes
    by_head = tuple(
        (
            jnp.moveaxis(item, 1, 0)
            for item in (x_act, write_heads, read_heads, head_step_sizes, logarithm_decay)
        )
    )
    head_outputs = jnp.moveaxis(lax.map(head_result, by_head), 0, 1)
    token_heads = lax.all_to_all(head_outputs, "sp", split_axis=0, concat_axis=1, tiled=True)
    gated_vals = token_heads.reshape(tok_rows, INNER).astype(jnp.float32) * jax.nn.silu(
        output_gate[0].astype(jnp.float32)
    )
    grouped = gated_vals.reshape(tok_rows, GROUPS, -1)
    grouped = grouped * lax.rsqrt(jnp.mean(grouped * grouped, axis=-1, keepdims=True) + EPS)
    normed = (grouped.reshape(tok_rows, -1) * grouped_norm_gain).astype(jnp.bfloat16)
    projected = jnp.dot(
        normed,
        lax.all_gather(output_matrix, "dp", axis=1, tiled=True),
        preferred_element_type=jnp.float32,
    )
    resid_one = (resid[0].astype(jnp.float32) + rms_scale(projected, output_gain)).astype(
        jnp.bfloat16
    )
    ffn_in = rms_scale(resid_one.astype(jnp.float32), feedforward_gain).astype(jnp.bfloat16)
    sp_size = lax.axis_size("sp")
    local_experts = expert_gate_weight.shape[0]
    experts = local_experts * sp_size
    capacity = 3 * tok_rows * TOPK // (2 * experts)
    flat_route = routes[0].reshape(-1)
    one_hot = (flat_route[:, None] == jnp.arange(experts, dtype=jnp.int32)[None, :]).astype(
        jnp.int32
    )
    earlier = jnp.cumsum(one_hot, axis=0) - one_hot
    slot_pos = jnp.sum(earlier * one_hot, axis=1)
    slot_dest = flat_route * capacity + slot_pos
    source_tok = jnp.arange(tok_rows * TOPK, dtype=jnp.int32) // TOPK
    slot_token = jnp.full((experts * capacity,), tok_rows, jnp.int32).at[slot_dest].set(source_tok)
    padded_in = jnp.concatenate([ffn_in, jnp.zeros((1, D), jnp.bfloat16)], axis=0)
    send_rows = padded_in[slot_token].reshape(sp_size, local_experts, capacity, D)
    arrived = lax.all_to_all(send_rows, "sp", split_axis=0, concat_axis=0, tiled=True)
    gate_part = jnp.einsum(
        "sekd,edh->sekh", arrived, expert_gate_weight, preferred_element_type=jnp.float32
    )
    up_part = jnp.einsum(
        "sekd,edh->sekh", arrived, expert_up_weight, preferred_element_type=jnp.float32
    )
    hidden = (jax.nn.silu(gate_part) * up_part).astype(jnp.bfloat16)
    expert_rows = jnp.einsum(
        "sekh,ehd->sekd", hidden, expert_down_weight, preferred_element_type=jnp.float32
    ).astype(jnp.bfloat16)
    returned = lax.all_to_all(expert_rows, "sp", split_axis=0, concat_axis=0, tiled=True)
    picked = returned.reshape(experts * capacity, D)[slot_dest]
    weighted = picked.astype(jnp.float32) * route_weights[0].reshape(-1)[:, None]
    combined = jnp.sum(weighted.reshape(tok_rows, TOPK, D), axis=1)
    mixed_out = resid_one.astype(jnp.float32) + rms_scale(combined, expert_sum_gain)
    return mixed_out.astype(jnp.bfloat16)[None]


def solution(mesh):
    in_specs = (
        P("dp", "sp", None),
        P("dp", "sp", None),
        P("dp", "sp", None),
        P("dp", "sp", None),
        P("dp", "sp", None),
        P("dp", "sp", None, None),
        P("dp", "sp", None, None),
        P(None, "sp"),
        P(),
        P(),
        P("sp", None),
        P("sp", None),
        P(),
        P(None, "dp"),
        P(),
        P(),
        P("dp", "sp", None),
        P("dp", "sp", None),
        P("sp", None, None),
        P("sp", None, None),
        P("sp", None, None),
        P(),
    )
    out_specs = P("dp", "sp", None)
    return jax.shard_map(local, mesh=mesh, in_specs=in_specs, out_specs=out_specs, check_vma=False)
```

profile of v0, /device:TPU:0, one launch (start us, length us, event | category | flops | bytes accessed | tf_op | source)
XLA Modules:
  0.0 578.3 jit_solution(10283695238567507477)
XLA Ops:
  8.0 14.2 %all_to_all.46 = bf16[256,64,2]{0,2,1:T(2,128)(2,1)S(1)} all-to-all(bf16[256,64,2]{0,2,1:T(2,128)(2,1)} %bitcast.401), channel_id=1, replica_groups=mesh['sp'=8,'dp'=4] {'sp'}, dimensions={1} | all-to-all | bytes 131072 | tf_op jit(solution)/shard_map/all_to_all | solution.py:114
  22.2 3.4 all-to-all-start.1
  25.6 4.1 copy.122
  29.7 2.8 all-to-all-done.1
  32.5 3.6 all-to-all-start.2
  38.6 24.9 %all-gather.10.cloned.1.call-done = bf16[1,2048,256]{2,1,0:T(8,128)(2,1)} async-done(((bf16[1,256,256]{2,1,0:T(8,128)(2,1)}), bf16[1,2048,256]{2,1,0:T(8,128)(2,1)}) %all-gather.10.cloned.1.call-update) | async-done | bytes 1048592 | tf_op jit(solution)/shard_map/all_gather | solution.py:118
  63.5 50.5 %all-gather.8.cloned.1.call-done = bf16[1,2048,256]{2,1,0:T(8,128)(2,1)} async-done(((bf16[1,256,256]{2,1,0:T(8,128)(2,1)}), bf16[1,2048,256]{2,1,0:T(8,128)(2,1)}) %all-gather.8.cloned.1.call-update) | async-done | bytes 1048592 | tf_op jit(solution)/shard_map/all_gather | solution.py:119
  120.1 6.8 %multiply_convert_fusion.4 = bf16[2048,512]{0,1:T(8,128)(2,1)} fusion(f32[2048,512]{0,1:T(8,128)S(1)} %bitcast.384, f32[512]{0:T(512)S(1)} %bitcast.406, f32[512]{0:T(512)S(1)} %bitcast.407, f32[512]{0:T(512)S(1)} %bitcast.404, f32[512]{0:T(512)S(1)} %bitcast.405, f32[512]{0:T(512)S(1)} %bitcast.403), kind=kLoop, calls=%fused_computation.110 | loop fusion | flops 14680064 | bytes 6301696 | tf_op jit(solution)/shard_map/convert_element_type | solution.py:29
  126.9 3.0 transpose.107
  129.9 2.6 transpose.108
  132.5 142.8 %while.10 = (s32[]{:T(128)}, bf16[8,2048,64]{1,2,0:T(8,128)(2,1)}, bf16[8,2048,128]{2,1,0:T(8,128)(2,1)}, bf16[8,2048,128]{2,1,0:T(8,128)(2,1)}, f32[8,2048,2]{1...) while((s32[]{:T(128)}, bf16[8,2048,64]{1,2,0:T(8,128)(2,1)}, ...), condition=%wide.region_5.6_spmd, body=%wide.region_0.5_spmd.sunk | while | flops 392190464 | bytes 29739348 | solution.py:142
  275.4 5.6 copy.124
  281.0 7.6 %reshape.357 = bf16[8,2,65536]{2,1,0:T(2,128)(2,1)} reshape(bf16[2048,8,64]{2,1,0:T(8,128)(2,1)} %bitcast.383) | data formatting | bytes 4194304
  288.5 4.7 all-to-all-start.3
  293.7 3.3 copy.127
  297.0 2.5 convert.66
  303.7 36.9 %all-to-all-done.3 = bf16[8,2,65536]{2,1,0:T(2,128)(2,1)} async-done(((bf16[8,2,65536]{2,1,0:T(2,128)(2,1)}), bf16[8,2,65536]{2,1,0:T(2,128)(2,1)}, u32[]{:S(2)}, u32[]{:S(2)}) %all-to-all-start.3) | async-done | bytes 2097184 | tf_op jit(solution)/shard_map/all_to_all | solution.py:143
  340.6 7.4 %reshape.358 = bf16[2048,8,64]{2,1,0:T(8,128)(2,1)} reshape(bf16[8,2,65536]{2,1,0:T(2,128)(2,1)} %all-to-all-done.3) | data formatting | bytes 4194304
  348.0 5.5 copy.125
  359.6 3.4 multiply_reduce_fusion.1
  363.0 3.5 copy.126
  366.6 2.8 fusion.72
  369.4 9.4 %multiply_reduce_fusion.3 = (f32[256]{0:T(256)S(1)}, f32[256,2048]{1,0:T(8,128)S(1)}) fusion(bf16[256,4096]{0,1:T(8,128)(2,1)} %fusion.72, bf16[4096,2048]{1,0:T(8,128)(2,1)} %all-gather.6.cloned.1.call-done), kind=kOutput, calls=%fused_computation.134 | convolution fusion | flops 4296015872 | bytes 20972544 | tf_op jit(solution)/shard_map/dot_general | solution.py:150
  380.8 4.3 gather_fusion
  385.1 74.7 %all_to_all.47 = bf16[8,1,96,2048]{3,2,1,0:T(8,128)(2,1)S(1)} all-to-all(bf16[8,1,96,2048]{3,2,1,0:T(8,128)(2,1)} %bitcast.387), channel_id=1, replica_groups=mesh['sp'=8,'dp'=4] {'sp'}, dimensions={0} | all-to-all | bytes 6291456 | tf_op jit(solution)/shard_map/all_to_all | solution.py:174
  459.8 5.1 fusion.67
  465.0 13.0 %fusion.87 = bf16[8,1,96,2048]{3,2,1,0:T(8,128)(2,1)} fusion(bf16[1,1024,2048]{2,1,0:T(8,128)(2,1)} %param.44, f32[8,96,1024]{2,1,0:T(8,128)} %fusion.67, bf16[1,2048,1024]{2,1,0:T(8,128)(2,1)} %param.42, bf16[8,1,96,2048]{3,2,1,0:T(8,128)(2,1)S(1)} %all_to_all.47), kind=kOutput, calls=%fused_computation.126 | convolution fusion | flops 6448742400 | bytes 17825792 | tf_op jit(solution)/shard_map/sekh,ehd->sekd/dot_general | solution.py:182
  478.0 4.0 all-to-all-start.5
  482.1 70.1 %all-to-all-done.5 = bf16[8,1,96,2048]{3,2,1,0:T(8,128)(2,1)S(1)} async-done(((bf16[8,1,96,2048]{3,2,1,0:T(8,128)(2,1)}), bf16[8,1,96,2048]{3,2,1,0:T(8,128)(2,1)S(1)}, u32[]{:S(2)}, u32[]{:S(2)}) %all-to-all-start.5) | async-done | bytes 3145760 | tf_op jit(solution)/shard_map/all_to_all | solution.py:185
  552.3 3.3 gather_fusion.1
  555.6 5.4 reshape.306
  561.0 9.0 %multiply_reduce_fusion = f32[256,2048]{1,0:T(8,128)S(1)} fusion(f32[256,2,2048]{2,1,0:T(2,128)} %reshape.306, f32[256,2]{1,0:T(8,128)S(1)} %copy.135), kind=kLoop, calls=%fused_computation.108 | loop fusion | flops 1572864 | bytes 6293504 | tf_op jit(solution)/shard_map/reduce_sum | solution.py:188
  (427 shorter events, 166.1 us)
Async XLA Ops:
  6.5 56.9 %all-gather.10.cloned.1.call-start = ((), (), s32[]{:S(2)}) async-start(), calls=%async_computation.8 | async-start | bytes 1179648 | tf_op jit(solution)/shard_map/all_gather | solution.py:118
  7.3 106.7 %all-gather.8.cloned.1.call-start = ((), (), s32[]{:S(2)}) async-start(), calls=%async_computation.7 | async-start | bytes 1179648 | tf_op jit(solution)/shard_map/all_gather | solution.py:119
  22.2 10.3 %all-to-all-start.1 = ((bf16[256,64,2]{0,2,1:T(2,128)(2,1)}), bf16[256,64,2]{0,2,1:T(2,128)(2,1)S(1)}, u32[]{:S(2)}, u32[]{:S(2)}) async-start(bf16[256,64,2]{0,2,1:T(2,128)(2,1)} %bitcast.402), calls=%async_computation.1 | async-start | bytes 131072 | tf_op jit(solution)/shard_map/all_to_all | solution.py:113
  32.5 84.4 %all-to-all-start.2 = ((bf16[256,64,64]{0,2,1:T(8,128)(2,1)}), bf16[256,64,64]{0,2,1:T(8,128)(2,1)S(1)}, u32[]{:S(2)}, u32[]{:S(2)}) async-start(bf16[256,64,64]{0,2,1:T(8,128)(2,1)} %bitcast.389), calls=%async_computation.2 | async-start | bytes 4194304 | tf_op jit(solution)/shard_map/all_to_all | solution.py:112
  36.1 0.8 copy-start.15
  36.1 0.9 copy-start.16
  36.1 1.0 copy-start.13
  36.2 1.0 copy-start.14
  36.2 1.0 copy-start.7
  36.2 333.2 %all-gather.6.cloned.1.call-start = ((), (), s32[]{:S(2)}) async-start(), calls=%async_computation.6 | async-start | bytes 20971520 | tf_op jit(solution)/shard_map/all_gather | solution.py:152
  147.4 2.2 copy-start.2
  165.3 2.2 copy-start.2
  183.2 2.2 copy-start.2
  201.0 2.2 copy-start.2
  218.9 2.2 copy-start.2
  236.7 2.2 copy-start.2
  254.5 2.2 copy-start.2
  272.4 2.2 copy-start.2
  288.5 4.7 copy-start.11
  288.5 52.0 %all-to-all-start.3 = ((bf16[8,2,65536]{2,1,0:T(2,128)(2,1)}), bf16[8,2,65536]{2,1,0:T(2,128)(2,1)}, u32[]{:S(2)}, u32[]{:S(2)}) async-start(bf16[8,2,65536]{2,1,0:T(2,128)(2,1)} %reshape.357), calls=%async_computation.3 | async-start | bytes 4194304 | tf_op jit(solution)/shard_map/all_to_all | solution.py:143
  355.6 4.0 copy-start.1
  357.6 2.0 copy-start
  363.0 3.6 copy-start.6
  369.4 9.4 %copy-start.5 = (bf16[1,256,2048]{2,1,0:T(8,128)(2,1)S(1)}, bf16[1,256,2048]{2,1,0:T(8,128)(2,1)}, u32[]{:S(2)}) copy-start(bf16[1,256,2048]{2,1,0:T(8,128)(2,1)} %param.24) | copy-start | bytes 3145732
  369.4 9.4 %copy-start.8 = (f32[2048]{0:T(1024)S(1)}, f32[2048]{0:T(1024)}, u32[]{:S(2)}) copy-start(f32[2048]{0:T(1024)} %param.38) | copy-start | bytes 24580
  378.8 1.6 copy-start.9
  379.5 1.0 copy-start.3
  385.1 74.7 %copy-start.17 = (bf16[1,2048,1024]{2,1,0:T(8,128)(2,1)S(1)}, bf16[1,2048,1024]{2,1,0:T(8,128)(2,1)}, u32[]{:S(2)}) copy-start(bf16[1,2048,1024]{2,1,0:T(8,128)(2,1)} %param.43) | copy-start | bytes 12582916
  478.0 4.0 copy-start.12
  478.0 74.3 %all-to-all-start.5 = ((bf16[8,1,96,2048]{3,2,1,0:T(8,128)(2,1)}), bf16[8,1,96,2048]{3,2,1,0:T(8,128)(2,1)S(1)}, u32[]{:S(2)}, u32[]{:S(2)}) async-start(bf16[8,1,96,2048]{3,2,1,0:T(8,128)(2,1)} %fusion.87), calls=%async_computation.5 | async-start | bytes 6291456 | tf_op jit(solution)/shard_map/all_to_all | solution.py:185
  561.0 9.2 %copy-start.4 = (bf16[256,2048]{1,0:T(8,128)(2,1)S(1)}, bf16[256,2048]{1,0:T(8,128)(2,1)}, u32[]{:S(2)}) copy-start(bf16[256,2048]{1,0:T(8,128)(2,1)} %copy-done.3) | copy-start | bytes 3145732
  561.0 9.2 %copy-start.10 = (f32[2048]{0:T(1024)S(1)}, f32[2048]{0:T(1024)}, u32[]{:S(2)}) copy-start(f32[2048]{0:T(1024)} %param.45) | copy-start | bytes 24580
Sparse Core Ops, SparseCore 0:
  9.5 53.9 all-gather.9
  65.6 48.3 all-gather.7
  115.5 104.5 all-gather.5
where the time goes:
time: 586 us; the launch traced here: 578 us
  waiting for transfers between devices  187 us (32%)
  local copies, waits for them, and re-layouts  144 us (25%)
  blocking collectives  89 us (15%)
  matrix products  77.1 us (13%)
  other arithmetic  50.6 us (9%)
  starting transfers between devices  15.7 us (3%)
  between operations  13.8 us (2%)
    all_to_all x1, blocking collectives, local(): lax.all_to_all(send_rows, 'sp', split_axis=0, concat_axis=0, tiled=True)  74.7 us
    all_to_all x1, waiting for transfers between devices, local(): lax.all_to_all(expert_rows, 'sp', split_axis=0, concat_axis=0, tiled=True)  70.1 us
    all_gather x1, waiting for transfers between devices, local(): lax.all_gather(read_rows_input[0], 'sp', axis=0, tiled=True)  50.5 us
    all_to_all x1, waiting for transfers between devices, local(): lax.all_to_all(head_outputs, 'sp', split_axis=0, concat_axis=1, tiled=True)  36.9 us
    unnamed x43, local copies, waits for them, and re-layouts  29.6 us
    all_gather x1, waiting for transfers between devices, local(): lax.all_gather(write_rows_input[0], 'sp', axis=0, tiled=True)  24.9 us
    dot_general x16, matrix products, block_pass(): jnp.einsum('cls,csp->clp', weights, inp_block, preferred_element_type=jnp...  19.8 us
    all_to_all x1, blocking collectives, local(): lax.all_to_all(extra_log_decay[0], 'sp', split_axis=1, concat_axis=0, til...  14.2 us
  transfers between devices with their start and end apart: 7, of which 5 were waited for; matrix products, arithmetic and copies ran while one was open for 37% of the time, Pallas kernels for 0%

commit v1 on v0

--- a/solution.py
+++ b/solution.py
@@ -140,7 +140,9 @@
         )
     )
     head_outputs = jnp.moveaxis(lax.map(head_result, by_head), 0, 1)
-    token_heads = lax.all_to_all(head_outputs, "sp", split_axis=0, concat_axis=1, tiled=True)
+    frame_out = jnp.split(head_outputs, lax.axis_size("sp"), axis=0)
+    mixed_arr = lax.all_to_all(jnp.stack(frame_out), axis_name="sp", split_axis=0, concat_axis=0)
+    token_heads = jnp.concatenate(mixed_arr, axis=1)
     gated_vals = token_heads.reshape(tok_rows, INNER).astype(jnp.float32) * jax.nn.silu(
         output_gate[0].astype(jnp.float32)
     )

time: 586 us -> 563 us (0.961)
  local copies, waits for them, and re-layouts: 144 us -> 125 us
    unnamed x43, local copies, waits for them, and re-layouts: 29.6 us -> 23.2 us
    while x33 -> x32, local copies, waits for them, and re-layouts: 14.1 us -> 8.43 us
  transfers between devices with their start and end apart: 7 -> 7, of which waited for: 5 -> 5; matrix products, arithmetic and copies ran while one was open for 37% -> 35% of each run, Pallas kernels for 0% -> 0%
where the time goes in v1:
time: 563 us; the launch traced here: 556 us
  waiting for transfers between devices  189 us (34%)
  local copies, waits for them, and re-layouts  125 us (22%)
  blocking collectives  89.2 us (16%)
  matrix products  76.6 us (14%)
  other arithmetic  47 us (8%)
  starting transfers between devices  15 us (3%)
  between operations  13.8 us (2%)
    all_to_all x1, blocking collectives, local(): lax.all_to_all(send_rows, 'sp', split_axis=0, concat_axis=0, tiled=True)  74.9 us
    all_to_all x1, waiting for transfers between devices, local(): lax.all_to_all(expert_rows, 'sp', split_axis=0, concat_axis=0, tiled=True)  70.1 us
    all_gather x1, waiting for transfers between devices, local(): lax.all_gather(read_rows_input[0], 'sp', axis=0, tiled=True)  50.5 us
    all_to_all x1, waiting for transfers between devices, local(): lax.all_to_all(jnp.stack(frame_out), axis_name='sp', split_axis=0, concat...  38.1 us
    all_gather x1, waiting for transfers between devices, local(): lax.all_gather(write_rows_input[0], 'sp', axis=0, tiled=True)  24.9 us
    unnamed x43, local copies, waits for them, and re-layouts  23.2 us
    dot_general x16, matrix products, block_pass(): jnp.einsum('cls,csp->clp', weights, inp_block, preferred_element_type=jnp...  19.8 us
    all_to_all x1, blocking collectives, local(): lax.all_to_all(extra_log_decay[0], 'sp', split_axis=1, concat_axis=0, til...  14.2 us
  transfers between devices with their start and end apart: 7, of which 5 were waited for; matrix products, arithmetic and copies ran while one was open for 35% of the time, Pallas kernels for 0%

profile of v1, /device:TPU:0, one launch (start us, length us, event | category | flops | bytes accessed | tf_op | source)
XLA Modules:
  0.0 555.8 jit_solution(7177205188583301503)
XLA Ops:
  8.0 14.2 %all_to_all.42 = bf16[256,64,2]{0,2,1:T(2,128)(2,1)S(1)} all-to-all(bf16[256,64,2]{0,2,1:T(2,128)(2,1)} %bitcast.433), channel_id=1, replica_groups=mesh['sp'=8,'dp'=4] {'sp'}, dimensions={1} | all-to-all | bytes 131072 | tf_op jit(solution)/shard_map/all_to_all | solution.py:114
  22.2 3.4 all-to-all-start.1
  25.6 4.1 copy.63
  29.7 2.8 all-to-all-done.1
  32.5 3.6 all-to-all-start.2
  38.6 24.9 %all-gather.10.cloned.1.call-done = bf16[1,2048,256]{2,1,0:T(8,128)(2,1)} async-done(((bf16[1,256,256]{2,1,0:T(8,128)(2,1)}), bf16[1,2048,256]{2,1,0:T(8,128)(2,1)}) %all-gather.10.cloned.1.call-update) | async-done | bytes 1048592 | tf_op jit(solution)/shard_map/all_gather | solution.py:118
  63.5 50.5 %all-gather.8.cloned.1.call-done = bf16[1,2048,256]{2,1,0:T(8,128)(2,1)} async-done(((bf16[1,256,256]{2,1,0:T(8,128)(2,1)}), bf16[1,2048,256]{2,1,0:T(8,128)(2,1)}) %all-gather.8.cloned.1.call-update) | async-done | bytes 1048592 | tf_op jit(solution)/shard_map/all_gather | solution.py:119
  118.1 2.0 copy.78
  120.1 7.1 %multiply_convert_fusion.4 = bf16[2048,512]{0,1:T(8,128)(2,1)} fusion(f32[2048,512]{0,1:T(8,128)S(1)} %bitcast.409, f32[512]{0:T(512)S(1)} %bitcast.438, f32[512]{0:T(512)S(1)} %bitcast.439, f32[512]{0:T(512)S(1)} %bitcast.436, f32[512]{0:T(512)S(1)} %bitcast.437, f32[512]{0:T(512)S(1)} %bitcast.435), kind=kLoop, calls=%fused_computation.112 | loop fusion | flops 14680064 | bytes 6301696 | tf_op jit(solution)/shard_map/convert_element_type | solution.py:29
  127.2 3.3 transpose.107
  130.5 2.5 transpose.108
  133.0 142.8 %while.10 = (s32[]{:T(128)}, bf16[8,2048,64]{1,2,0:T(8,128)(2,1)}, bf16[8,2048,128]{2,1,0:T(8,128)(2,1)}, bf16[8,2048,128]{2,1,0:T(8,128)(2,1)}, f32[8,2048,2]{1...) while((s32[]{:T(128)}, bf16[8,2048,64]{1,2,0:T(8,128)(2,1)}, ...), condition=%wide.region_5.6_spmd, body=%wide.region_0.5_spmd.sunk | while | flops 392190464 | bytes 29739348 | solution.py:142
  282.4 1.7 fusion.116
  284.1 1.7 fusion.115
  285.8 1.7 fusion.114
  287.5 1.7 fusion.113
  289.2 3.9 all-to-all-start.3
  293.5 4.1 copy.65
  299.4 2.4 scatter_custom_fusion
  301.9 38.1 %all-to-all-done.3 = bf16[8,256,8,64]{1,3,2,0:T(8,128)(2,1)S(1)} async-done(((bf16[8,256,8,64]{1,3,2,0:T(8,128)(2,1)}), bf16[8,256,8,64]{1,3,2,0:T(8,128)(2,1)S(1)}, u32[]{:S(2)}, u32[]{:S(2)}) %all-to-all-start.3) | async-done | bytes 2097184 | tf_op jit(solution)/shard_map/all_to_all | solution.py:144
  340.0 3.2 fusion.78
  343.2 3.7 fusion.67
  347.0 9.0 %multiply_reduce_fusion.2 = (f32[256]{0:T(256)S(1)}, f32[256,2048]{1,0:T(8,128)S(1)}) fusion(bf16[256,4096]{0,1:T(8,128)(2,1)} %fusion.67, bf16[4096,2048]{1,0:T(8,128)(2,1)} %all-gather.6.cloned.1.call-done), kind=kOutput, calls=%fused_computation.136 | convolution fusion | flops 4296015872 | bytes 20972544 | tf_op jit(solution)/shard_map/dot_general | solution.py:152
  358.0 4.3 gather_fusion
  362.3 74.9 %all_to_all.43 = bf16[8,1,96,2048]{3,2,1,0:T(8,128)(2,1)S(1)} all-to-all(bf16[8,1,96,2048]{3,2,1,0:T(8,128)(2,1)} %bitcast.411), channel_id=1, replica_groups=mesh['sp'=8,'dp'=4] {'sp'}, dimensions={0} | all-to-all | bytes 6291456 | tf_op jit(solution)/shard_map/all_to_all | solution.py:176
  437.2 5.1 fusion.70
  442.3 13.0 %fusion.89 = bf16[8,1,96,2048]{3,2,1,0:T(8,128)(2,1)} fusion(bf16[1,1024,2048]{2,1,0:T(8,128)(2,1)} %param.44, f32[8,96,1024]{2,1,0:T(8,128)} %fusion.70, bf16[1,2048,1024]{2,1,0:T(8,128)(2,1)} %param.42, bf16[8,1,96,2048]{3,2,1,0:T(8,128)(2,1)S(1)} %all_to_all.43), kind=kOutput, calls=%fused_computation.128 | convolution fusion | flops 6448742400 | bytes 17825792 | tf_op jit(solution)/shard_map/sekh,ehd->sekd/dot_general | solution.py:184
  455.3 4.1 all-to-all-start.5
  459.5 70.1 %all-to-all-done.5 = bf16[8,1,96,2048]{3,2,1,0:T(8,128)(2,1)S(1)} async-done(((bf16[8,1,96,2048]{3,2,1,0:T(8,128)(2,1)}), bf16[8,1,96,2048]{3,2,1,0:T(8,128)(2,1)S(1)}, u32[]{:S(2)}, u32[]{:S(2)}) %all-to-all-start.5) | async-done | bytes 3145760 | tf_op jit(solution)/shard_map/all_to_all | solution.py:187
  529.7 3.3 gather_fusion.1
  533.0 5.4 reshape.301
  538.4 9.0 %multiply_reduce_fusion = f32[256,2048]{1,0:T(8,128)S(1)} fusion(f32[256,2,2048]{2,1,0:T(2,128)} %reshape.301, f32[256,2]{1,0:T(8,128)S(1)} %copy.71), kind=kLoop, calls=%fused_computation.111 | loop fusion | flops 1572864 | bytes 6293504 | tf_op jit(solution)/shard_map/reduce_sum | solution.py:190
  (423 shorter events, 162.2 us)
Async XLA Ops:
  6.5 56.9 %all-gather.10.cloned.1.call-start = ((), (), s32[]{:S(2)}) async-start(), calls=%async_computation.8 | async-start | bytes 1179648 | tf_op jit(solution)/shard_map/all_gather | solution.py:118
  7.3 106.7 %all-gather.8.cloned.1.call-start = ((), (), s32[]{:S(2)}) async-start(), calls=%async_computation.7 | async-start | bytes 1179648 | tf_op jit(solution)/shard_map/all_gather | solution.py:119
  22.2 10.3 %all-to-all-start.1 = ((bf16[256,64,2]{0,2,1:T(2,128)(2,1)}), bf16[256,64,2]{0,2,1:T(2,128)(2,1)S(1)}, u32[]{:S(2)}, u32[]{:S(2)}) async-start(bf16[256,64,2]{0,2,1:T(2,128)(2,1)} %bitcast.434), calls=%async_computation.1 | async-start | bytes 131072 | tf_op jit(solution)/shard_map/all_to_all | solution.py:113
  32.5 84.4 %all-to-all-start.2 = ((bf16[256,64,64]{0,2,1:T(8,128)(2,1)}), bf16[256,64,64]{0,2,1:T(8,128)(2,1)S(1)}, u32[]{:S(2)}, u32[]{:S(2)}) async-start(bf16[256,64,64]{0,2,1:T(8,128)(2,1)} %bitcast.413), calls=%async_computation.2 | async-start | bytes 4194304 | tf_op jit(solution)/shard_map/all_to_all | solution.py:112
  36.1 0.8 copy-start.13
  36.1 0.9 copy-start.14
  36.1 1.0 copy-start.11
  36.2 1.0 copy-start.12
  36.2 1.0 copy-start.5
  36.2 310.8 %all-gather.6.cloned.1.call-start = ((), (), s32[]{:S(2)}) async-start(), calls=%async_computation.6 | async-start | bytes 20971520 | tf_op jit(solution)/shard_map/all_gather | solution.py:154
  147.9 2.2 copy-start
  165.8 2.2 copy-start
  183.6 2.2 copy-start
  201.5 2.2 copy-start
  219.3 2.2 copy-start
  237.1 2.2 copy-start
  255.0 2.2 copy-start
  272.8 2.2 copy-start
  282.4 10.6 %copy-start.9 = (s32[1,256,2]{1,2,0:T(2,128)S(1)}, s32[1,256,2]{1,2,0:T(2,128)}, u32[]{:S(2)}) copy-start(s32[1,256,2]{1,2,0:T(2,128)} %param.40) | copy-start | bytes 6148
  289.2 50.8 %all-to-all-start.3 = ((bf16[8,256,8,64]{1,3,2,0:T(8,128)(2,1)}), bf16[8,256,8,64]{1,3,2,0:T(8,128)(2,1)S(1)}, u32[]{:S(2)}, u32[]{:S(2)}) async-start(bf16[8,256,8,64]{1,3,2,0:T(8,128)(2,1)} %fusion.113), calls=%async_computation.3 | async-start | bytes 4194304 | tf_op jit(solution)/shard_map/all_to_all | solution.py:144
  297.6 45.6 %copy-start.4 = (f32[4096]{0:T(1024)S(1)}, f32[4096]{0:T(1024)}, u32[]{:S(2)}) copy-start(f32[4096]{0:T(1024)} %param.36) | copy-start | bytes 49156
  347.0 9.0 %copy-start.3 = (bf16[1,256,2048]{2,1,0:T(8,128)(2,1)S(1)}, bf16[1,256,2048]{2,1,0:T(8,128)(2,1)}, u32[]{:S(2)}) copy-start(bf16[1,256,2048]{2,1,0:T(8,128)(2,1)} %param.24) | copy-start | bytes 3145732
  347.0 9.0 %copy-start.6 = (f32[2048]{0:T(1024)S(1)}, f32[2048]{0:T(1024)}, u32[]{:S(2)}) copy-start(f32[2048]{0:T(1024)} %param.38) | copy-start | bytes 24580
  356.0 1.6 copy-start.7
  356.6 1.0 copy-start.1
  362.2 74.9 %copy-start.15 = (bf16[1,2048,1024]{2,1,0:T(8,128)(2,1)S(1)}, bf16[1,2048,1024]{2,1,0:T(8,128)(2,1)}, u32[]{:S(2)}) copy-start(bf16[1,2048,1024]{2,1,0:T(8,128)(2,1)} %param.43) | copy-start | bytes 12582916
  455.3 4.1 copy-start.10
  455.3 74.4 %all-to-all-start.5 = ((bf16[8,1,96,2048]{3,2,1,0:T(8,128)(2,1)}), bf16[8,1,96,2048]{3,2,1,0:T(8,128)(2,1)S(1)}, u32[]{:S(2)}, u32[]{:S(2)}) async-start(bf16[8,1,96,2048]{3,2,1,0:T(8,128)(2,1)} %fusion.89), calls=%async_computation.5 | async-start | bytes 6291456 | tf_op jit(solution)/shard_map/all_to_all | solution.py:187
  538.4 9.2 %copy-start.2 = (bf16[256,2048]{1,0:T(8,128)(2,1)S(1)}, bf16[256,2048]{1,0:T(8,128)(2,1)}, u32[]{:S(2)}) copy-start(bf16[256,2048]{1,0:T(8,128)(2,1)} %copy-done.1) | copy-start | bytes 3145732
  538.4 9.2 %copy-start.8 = (f32[2048]{0:T(1024)S(1)}, f32[2048]{0:T(1024)}, u32[]{:S(2)}) copy-start(f32[2048]{0:T(1024)} %param.45) | copy-start | bytes 24580
Sparse Core Ops, SparseCore 0:
  9.5 53.9 all-gather.9
  65.6 48.3 all-gather.7
  115.5 104.5 all-gather.5
